TPU v7x, 32 devices: a whole 2x2x4 slice. The times are simulated.
32 devices in a mesh: rep: 2 (over x), fs: 8 (over z, y), tp: 2 (over core).
Axes of the slice: x: 2, y: 2, z: 4, core: 2. Of those that a mesh axis runs over, the one named last changes fastest.
Arguments:
- inputs: bfloat16 [6144, 2048], P(('rep', 'fs')), may hold values from -6 to 6
- w_up: bfloat16 [2048, 4096], P('fs', 'tp'), may hold values from -0.125 to 0.125
- w_down: bfloat16 [4096, 2048], P('tp', 'fs'), may hold values from -0.09375 to 0.09375
- cotangent: bfloat16 [6144, 2048], P(('rep', 'fs')), may hold values from -6 to 6
Outputs:
- d_inputs: bfloat16 [6144, 2048], P(('rep', 'fs'))
- d_w_up: float32 [2048, 4096], P('fs', 'tp')
All inputs are finite; a program needn't handle non-finite values.
Results may differ from a plain program's by a relative error of at most 0.014.
Values may be sent and summed in bfloat16 or wider, within the bound.
A program may use at most 128 MiB of HBM per device.

v0:
```python
import jax
import jax.numpy as jnp
from jax import lax
from jax.sharding import PartitionSpec as P


def per_device(inputs, w_up, w_down, cotangent):
    up_whole = lax.all_gather(w_up, "fs", axis=0, tiled=True)
    preact = jnp.dot(inputs, up_whole, preferred_element_type=jnp.float32)
    columns = cotangent
    grad_hidden = lax.dot_general(
        columns,
        lax.all_gather(w_down, "fs", axis=1, tiled=True),
        (((1,), (1,)), ((), ())),
        preferred_element_type=jnp.float32,
    )
    grad_pre = (2.0 * jnp.maximum(preact, 0.0) * grad_hidden).astype(jnp.bfloat16)
    partial_value = lax.dot_general(
        grad_pre, up_whole, (((1,), (1,)), ((), ())), preferred_element_type=jnp.float32
    )
    d_inputs = lax.psum(partial_value.astype(jnp.bfloat16), "tp")
    columns = inputs
    own_rows = lax.psum_scatter(
        lax.dot_general(
            columns, grad_pre, (((0,), (0,)), ((), ())), preferred_element_type=jnp.float32
        ),
        "fs",
        scatter_dimension=0,
        tiled=True,
    )
    d_w_up = lax.psum(own_rows, "rep")
    return (d_inputs, d_w_up)


def solution(mesh):
    in_specs = (P(("rep", "fs"), None), P("fs", "tp"), P("tp", "fs"), P(("rep", "fs"), None))
    out_specs = (P(("rep", "fs"), None), P("fs", "tp"))
    return jax.shard_map(
        per_device, mesh=mesh, in_specs=in_specs, out_specs=out_specs, check_vma=False
    )
```

profile of v0, /device:TPU:0, one launch (start us, length us, event | category | flops | bytes accessed | tf_op | source)
XLA Modules:
  0.0 653.7 jit_solution(10477161835082296149)
XLA Ops:
  7.2 0.0 copy-start
  7.2 0.0 all-gather.5.cloned.1.call-start
  7.2 0.7 all-gather.5.cloned.1.call-update
  7.9 0.0 all-gather.3.cloned.1.call-start
  8.0 0.7 all-gather.3.cloned.1.call-update
  8.7 0.0 reduce-scatter.2.cloned.1.call-start
  8.7 129.0 %all-gather.5.cloned.1.call-done = bf16[2048,2048]{1,0:T(8,128)(2,1)} async-done(((bf16[2048,256]{1,0:T(8,128)(2,1)}), bf16[2048,2048]{1,0:T(8,128)(2,1)}) %all-gather.5.cloned.1.call-update) | async-done | bytes 8388624 | tf_op jit(solution)/shard_map/all_gather | solution.py:13
  137.7 9.0 %fusion.11 = f32[384,2048]{1,0:T(8,128)} fusion(bf16[384,2048]{1,0:T(8,128)(2,1)} %param.7, bf16[2048,2048]{1,0:T(8,128)(2,1)} %all-gather.5.cloned.1.call-done), kind=kOutput, calls=%fused_computation.13 | convolution fusion | flops 3221225472 | bytes 13107200 | tf_op jit(solution)/shard_map/dot_general | solution.py:11
  146.8 115.8 %all-gather.3.cloned.1.call-done = bf16[2048,2048]{1,0:T(8,128)(2,1)} async-done(((bf16[256,2048]{1,0:T(8,128)(2,1)}), bf16[2048,2048]{1,0:T(8,128)(2,1)}) %all-gather.3.cloned.1.call-update) | async-done | bytes 8388624 | tf_op jit(solution)/shard_map/all_gather | solution.py:8
  262.5 5.9 fusion.10
  268.5 0.0 copy-start.2
  268.5 1.7 copy-done.2
  270.2 8.3 %convolution_bitcast_fusion = f32[2048,2048]{0,1:T(8,128)} fusion(bf16[384,2048]{1,0:T(8,128)(2,1)S(1)} %copy-done, f32[384,2048]{1,0:T(8,128)S(1)} %copy-done.1, f32[384,2048]{1,0:T(8,128)S(1)} %fusion.10), kind=kOutput, calls=%fused_computation | convolution fusion | flops 3224371200 | bytes 24641536 | tf_op jit(solution)/shard_map/dot_general | solution.py:24
  278.5 0.0 reduce-scatter.2.cloned.1.call-update
  278.5 0.0 all-reduce.5.cloned.1.call-start
  278.6 278.5 %reduce-scatter.2.cloned.1.call-done = f32[256,2048]{0,1:T(8,128)} async-done(((f32[2048,2048]{0,1:T(8,128)}), f32[256,2048]{0,1:T(8,128)}) %reduce-scatter.2.cloned.1.call-update) | async-done | bytes 2097168 | tf_op jit(solution)/shard_map/reduce_scatter | solution.py:23
  557.1 0.0 all-reduce.5.cloned.1.call-update
  557.1 0.0 all-reduce.3.cloned.1.call-start
  557.2 9.8 %fusion.1 = bf16[384,2048]{1,0:T(8,128)(2,1)} fusion(bf16[2048,2048]{1,0:T(8,128)(2,1)} %all-gather.3.cloned.1.call-done, f32[384,2048]{1,0:T(8,128)} %fusion.11, f32[384,2048]{1,0:T(8,128)} %copy-done.2), kind=kOutput, calls=%fused_computation.3 | convolution fusion | flops 3225157632 | bytes 16252928 | tf_op jit(solution)/shard_map/dot_general | solution.py:18
  567.0 0.0 all-reduce.3.cloned.1.call-update
  567.0 54.3 %all-reduce.5.cloned.1.call-done = f32[256,2048]{0,1:T(8,128)} async-done(((f32[256,2048]{0,1:T(8,128)}), f32[256,2048]{0,1:T(8,128)}) %all-reduce.5.cloned.1.call-update) | async-done | bytes 2097168 | tf_op jit(solution)/shard_map/psum | solution.py:31
  621.3 2.9 copy.6
  624.2 20.3 %all-reduce.3.cloned.1.call-done = bf16[384,2048]{1,0:T(8,128)(2,1)} async-done(((bf16[384,2048]{1,0:T(8,128)(2,1)}), bf16[384,2048]{1,0:T(8,128)(2,1)}) %all-reduce.3.cloned.1.call-update) | async-done | bytes 1572880 | tf_op jit(solution)/shard_map/psum | solution.py:21
  644.5 2.7 copy.9
  (3 shorter events, 0.0 us)
Async XLA Ops:
  7.2 255.4 %copy-start = (bf16[384,2048]{1,0:T(8,128)(2,1)S(1)}, bf16[384,2048]{1,0:T(8,128)(2,1)}, u32[]{:S(2)}) copy-start(bf16[384,2048]{1,0:T(8,128)(2,1)} %param.4) | copy-start | bytes 4718596
  7.2 130.5 %all-gather.5.cloned.1.call-start = ((), (), s32[]{:S(2)}) async-start(), calls=%async_computation.2 | async-start | bytes 9437184 | tf_op jit(solution)/shard_map/all_gather | solution.py:13
  7.9 254.6 %all-gather.3.cloned.1.call-start = ((), (), s32[]{:S(2)}) async-start(), calls=%async_computation.1 | async-start | bytes 9437184 | tf_op jit(solution)/shard_map/all_gather | solution.py:8
  8.7 548.4 %reduce-scatter.2.cloned.1.call-start = ((), (), s32[]{:S(2)}) async-start(), calls=%async_computation.4 | async-start | bytes 18874368 | tf_op jit(solution)/shard_map/reduce_scatter | solution.py:23
  262.5 7.7 %copy-start.1 = (f32[384,2048]{1,0:T(8,128)S(1)}, f32[384,2048]{1,0:T(8,128)}, u32[]{:S(2)}) copy-start(f32[384,2048]{1,0:T(8,128)} %fusion.11) | copy-start | bytes 9437188
  268.5 1.7 copy-start.2
  278.5 342.8 %all-reduce.5.cloned.1.call-start = ((), (), s32[]{:S(2)}) async-start(), calls=%async_computation.5 | async-start | bytes 4194304 | tf_op jit(solution)/shard_map/psum | solution.py:31
  557.1 87.4 %all-reduce.3.cloned.1.call-start = ((), (), s32[]{:S(2)}) async-start(), calls=%async_computation.3 | async-start | bytes 3145728 | tf_op jit(solution)/shard_map/psum | solution.py:21
Sparse Core Ops, SparseCore 0:
  10.0 127.6 all-gather.4
  139.8 122.6 all-gather.2
  278.6 278.3 reduce-scatter.1
  559.2 62.0 all-reduce.4
  624.1 20.3 all-reduce.2
where the time goes:
time: 654 us
  waiting for transfers between devices  599 us (92%)
  matrix products  33.1 us (5%)
  between operations  13.8 us (2%)
  local copies, waits for them, and re-layouts  7.35 us (1%)
    reduce_scatter x1, waiting for transfers between devices, per_device(): lax.psum_scatter(lax.dot_general(columns, grad_pre, (((0,), (0,)), ((), (...  279 us
    all_gather x1, waiting for transfers between devices, per_device(): lax.all_gather(w_down, 'fs', axis=1, tiled=True)  129 us
    all_gather x1, waiting for transfers between devices, per_device(): up_whole = lax.all_gather(w_up, 'fs', axis=0, tiled=True)  116 us
    psum x1, waiting for transfers between devices, per_device(): d_w_up = lax.psum(own_rows, 'rep')  54.3 us
    psum x1, waiting for transfers between devices, per_device(): d_inputs = lax.psum(partial_value.astype(jnp.bfloat16), 'tp')  20.3 us
  transfers between devices with their start and end apart: 5, of which 5 were waited for; matrix products, arithmetic and copies ran while one was open for 3% of the time, Pallas kernels for 0%

commit v1 on v0

v1 whole, which is shorter than its diff:
```python
import jax
import jax.numpy as jnp
from jax import lax
from jax.sharding import PartitionSpec as P


def per_device(inputs, w_up, w_down, cotangent):
    n_rep = lax.axis_size("rep")
    rep = lax.axis_index("rep")
    tokens = inputs.shape[0]
    hidden = w_up.shape[1] // n_rep

    def from_rep(value, step):
        return lax.ppermute(value, "rep", [((r + step) % n_rep, r) for r in range(n_rep)])

    up_block = lax.dynamic_slice_in_dim(w_up, rep * hidden, hidden, axis=1)
    down_block = lax.dynamic_slice_in_dim(w_down, rep * hidden, hidden, axis=0)
    up_whole = lax.all_gather(up_block, "fs", axis=0, tiled=True)
    down_whole = lax.all_gather(down_block, "fs", axis=1, tiled=True)
    rows = jnp.concatenate([inputs] + [from_rep(inputs, k) for k in range(1, n_rep)], axis=0)
    cots = jnp.concatenate([cotangent] + [from_rep(cotangent, k) for k in range(1, n_rep)], axis=0)
    preact = jnp.dot(rows, up_whole, preferred_element_type=jnp.float32)
    grad_hidden = lax.dot_general(
        cots, down_whole, (((1,), (1,)), ((), ())), preferred_element_type=jnp.float32
    )
    grad_pre = (2.0 * jnp.maximum(preact, 0.0) * grad_hidden).astype(jnp.bfloat16)
    d_w = lax.dot_general(
        rows, grad_pre, (((0,), (0,)), ((), ())), preferred_element_type=jnp.float32
    ).astype(jnp.bfloat16)
    own_rows = lax.psum_scatter(d_w, "fs", scatter_dimension=0, tiled=True)
    partial_value = lax.dot_general(
        grad_pre, up_whole, (((1,), (1,)), ((), ())), preferred_element_type=jnp.float32
    )
    own = partial_value[:tokens]
    for k in range(1, n_rep):
        mine = partial_value[k * tokens:(k + 1) * tokens].astype(jnp.bfloat16)
        own = own + from_rep(mine, n_rep - k).astype(jnp.float32)
    d_inputs = lax.psum(own.astype(jnp.bfloat16), "tp")
    whole_rows = jnp.zeros((own_rows.shape[0], w_up.shape[1]), jnp.float32)
    for k in range(n_rep):
        block = own_rows if k == 0 else from_rep(own_rows, k)
        at = lax.rem(rep + k, n_rep) * hidden
        whole_rows = lax.dynamic_update_slice_in_dim(whole_rows, block.astype(jnp.float32), at, axis=1)
    return (d_inputs, whole_rows)


def solution(mesh):
    in_specs = (P(("rep", "fs"), None), P("fs", "tp"), P("tp", "fs"), P(("rep", "fs"), None))
    out_specs = (P(("rep", "fs"), None), P("fs", "tp"))
    return jax.shard_map(
        per_device, mesh=mesh, in_specs=in_specs, out_specs=out_specs, check_vma=False
    )
```

time: 654 us -> 296 us (0.45)
  waiting for transfers between devices: 599 us -> 232 us
    reduce_scatter x1, waiting for transfers between devices: 279 us -> 42.5 us  [per_device(): own_rows = lax.psum_scatter(d_w, 'fs', scatter_dimension=0, tiled=True)]
    all_gather x2, waiting for transfers between devices: 245 us -> 103 us  [the longest x1 67.5 us: per_device(): down_whole = lax.all_gather(down_block, 'fs', axis=1, tiled=True)]
    ppermute x0 -> x4, waiting for transfers between devices: none -> 78.5 us  [from_rep(): lax.ppermute(value, 'rep', [((r + step) % n_rep, r) for r in range(n_rep)])]
    psum x2 -> x1, waiting for transfers between devices: 74.6 us -> 8.01 us  [per_device(): d_inputs = lax.psum(own.astype(jnp.bfloat16), 'tp')]
  transfers between devices with their start and end apart: 5 -> 8, of which waited for: 5 -> 7; matrix products, arithmetic and copies ran while one was open for 3% -> 8% of each run, Pallas kernels for 0% -> 0%
where the time goes in v1:
time: 296 us
  waiting for transfers between devices  232 us (78%)
  matrix products  27.7 us (9%)
  between operations  13.9 us (5%)
  local copies, waits for them, and re-layouts  12.1 us (4%)
  starting transfers between devices  6.32 us (2%)
  other arithmetic  4.01 us (1%)
    ppermute x4, waiting for transfers between devices, from_rep(): lax.ppermute(value, 'rep', [((r + step) % n_rep, r) for r in range(n_rep)])  78.5 us
    all_gather x1, waiting for transfers between devices, per_device(): down_whole = lax.all_gather(down_block, 'fs', axis=1, tiled=True)  67.5 us
    reduce_scatter x1, waiting for transfers between devices, per_device(): own_rows = lax.psum_scatter(d_w, 'fs', scatter_dimension=0, tiled=True)  42.5 us
    all_gather x1, waiting for transfers between devices, per_device(): up_whole = lax.all_gather(up_block, 'fs', axis=0, tiled=True)  35.4 us
    dot_general x1, matrix products, per_device(): preact = jnp.dot(rows, up_whole, preferred_element_type=jnp.float32)  8.28 us
    psum x1, waiting for transfers between devices, per_device(): d_inputs = lax.psum(own.astype(jnp.bfloat16), 'tp')  8.01 us
    unnamed x14, local copies, waits for them, and re-layouts  7.72 us
    dot_general x1, matrix products, per_device(): lax.dot_general(cots, down_whole, (((1,), (1,)), ((), ())), preferred_ele...  7.07 us
  transfers between devices with their start and end apart: 8, of which 7 were waited for; matrix products, arithmetic and copies ran while one was open for 8% of the time, Pallas kernels for 0%

profile of v1, /device:TPU:0, one launch (start us, length us, event | category | flops | bytes accessed | tf_op | source)
XLA Modules:
  0.0 296.0 jit_solution(13149260380039072654)
XLA Ops:
  7.2 1.2 copy-done
  9.3 1.9 constant_dynamic-slice_fusion
  11.3 3.0 %collective-permute-start = (bf16[384,2048]{1,0:T(8,128)(2,1)S(1)}, bf16[384,2048]{1,0:T(8,128)(2,1)S(1)}, u32[]{:S(2)}, u32[]{:S(2)}) collective-permute-start(bf16[384,2048]{1,0:T(8,128)(2,1)S(1)} %copy-done.2), channel_id=1, source_target_pairs={{16,0},{0,16},{17,1},{1,17},{18,2},{2,18},{19,3},{3,19},{20,4},{4,... | collective-permute-start | bytes 4718600 | tf_op jit(solution)/shard_map/ppermute | solution.py:14
  14.4 1.3 constant_dynamic-update-slice_fusion.1
  15.7 33.8 %collective-permute-done = bf16[384,2048]{1,0:T(8,128)(2,1)S(1)} collective-permute-done((bf16[384,2048]{1,0:T(8,128)(2,1)S(1)}, bf16[384,2048]{1,0:T(8,128)(2,1)S(1)}, u32[]{:S(2)}, u32[]{:S(2)}) %collective-permute-start) | collective-permute-done | bytes 1572896 | tf_op jit(solution)/shard_map/ppermute | solution.py:14
  49.5 1.3 constant_dynamic-update-slice_fusion
  50.8 35.4 %all-gather.3.cloned.1.call-done = bf16[2048,1024]{1,0:T(8,128)(2,1)} async-done(((bf16[256,1024]{1,0:T(8,128)(2,1)}), bf16[2048,1024]{1,0:T(8,128)(2,1)}) %all-gather.3.cloned.1.call-update) | async-done | bytes 4194320 | tf_op jit(solution)/shard_map/all_gather | solution.py:18
  86.2 8.3 %fusion.8 = f32[768,1024]{1,0:T(8,128)} fusion(bf16[768,2048]{1,0:T(8,128)(2,1)} %constant_dynamic-update-slice_fusion, bf16[2048,1024]{1,0:T(8,128)(2,1)} %all-gather.3.cloned.1.call-done), kind=kOutput, calls=%fused_computation.16 | convolution fusion | flops 3221225472 | bytes 10485760 | tf_op jit(solution)/shard_map/dot_general | solution.py:22
  94.5 67.5 %all-gather.5.cloned.1.call-done = bf16[1024,2048]{1,0:T(8,128)(2,1)} async-done(((bf16[1024,256]{1,0:T(8,128)(2,1)}), bf16[1024,2048]{1,0:T(8,128)(2,1)}) %all-gather.5.cloned.1.call-update) | async-done | bytes 4194320 | tf_op jit(solution)/shard_map/all_gather | solution.py:19
  162.1 7.1 %multiply_convert_fusion = bf16[768,1024]{1,0:T(8,128)(2,1)S(1)} fusion(f32[768,1024]{1,0:T(8,128)} %fusion.8, bf16[1024,2048]{1,0:T(8,128)(2,1)} %all-gather.5.cloned.1.call-done, bf16[384,2048]{1,0:T(8,128)(2,1)} %collective-permute-done.1, bf16[384,2048]{1,0:T(8,128)(2,1)S(1)} %copy-done.3), kind=kOutput, calls=%fused_computation.8 | convolution fusion | flops 3230662656 | bytes 12058624 | tf_op jit(solution)/shard_map/dot_general | solution.py:23
  169.2 1.1 copy-done.4
  170.3 7.0 %convolution_convert_fusion = bf16[2048,1024]{1,0:T(8,128)(2,1)} fusion(bf16[768,2048]{1,0:T(8,128)(2,1)} %constant_dynamic-update-slice_fusion, bf16[768,1024]{1,0:T(8,128)(2,1)S(1)} %multiply_convert_fusion), kind=kOutput, calls=%fused_computation | convolution fusion | flops 3223322624 | bytes 8912896 | tf_op jit(solution)/shard_map/dot_general | solution.py:27
  177.4 1.3 copy-done.5
  178.7 5.3 %fusion.9 = f32[768,2048]{1,0:T(8,128)S(1)} fusion(bf16[768,1024]{1,0:T(8,128)(2,1)S(1)} %copy-done.5, bf16[2048,1024]{1,0:T(8,128)(2,1)} %all-gather.3.cloned.1.call-done), kind=kOutput, calls=%fused_computation.17 | convolution fusion | flops 3221225472 | bytes 12058624 | tf_op jit(solution)/shard_map/dot_general | solution.py:31
  184.2 1.6 collective-permute-start.2
  185.8 33.9 %collective-permute-done.2 = bf16[384,2048]{1,0:T(8,128)(2,1)S(1)} collective-permute-done((bf16[384,2048]{1,0:T(8,128)(2,1)S(1)}, bf16[384,2048]{1,0:T(8,128)(2,1)S(1)}, u32[]{:S(2)}, u32[]{:S(2)}) %collective-permute-start.2) | collective-permute-done | bytes 1572896 | tf_op jit(solution)/shard_map/ppermute | solution.py:14
  219.7 1.7 fusion
  221.4 42.5 %reduce-scatter.2.cloned.1.call-done = bf16[256,1024]{1,0:T(8,128)(2,1)} async-done(((bf16[2048,1024]{1,0:T(8,128)(2,1)}), bf16[256,1024]{1,0:T(8,128)(2,1)}) %reduce-scatter.2.cloned.1.call-update) | async-done | bytes 524304 | tf_op jit(solution)/shard_map/reduce_scatter | solution.py:30
  263.9 1.5 collective-permute-start.3
  265.6 1.2 convert_dynamic-update-slice_fusion.1
  266.8 10.8 %collective-permute-done.3 = bf16[256,1024]{1,0:T(8,128)(2,1)} collective-permute-done((bf16[256,1024]{1,0:T(8,128)(2,1)}, bf16[256,1024]{1,0:T(8,128)(2,1)}, u32[]{:S(2)}, u32[]{:S(2)}) %collective-permute-start.3) | collective-permute-done | bytes 524320 | tf_op jit(solution)/shard_map/ppermute | solution.py:14
  277.6 1.1 convert_dynamic-update-slice_fusion
  278.7 8.0 %all-reduce.2.cloned.1.call-done = bf16[384,2048]{1,0:T(8,128)(2,1)} async-done(((bf16[384,2048]{1,0:T(8,128)(2,1)}), bf16[384,2048]{1,0:T(8,128)(2,1)}) %all-reduce.2.cloned.1.call-update) | async-done | bytes 1572880 | tf_op jit(solution)/shard_map/psum | solution.py:38
  286.7 2.7 copy.10
  (22 shorter events, 1.6 us)
Async XLA Ops:
  7.2 1.2 copy-start
  7.2 4.1 %copy-start.2 = (bf16[384,2048]{1,0:T(8,128)(2,1)S(1)}, bf16[384,2048]{1,0:T(8,128)(2,1)}, u32[]{:S(2)}) copy-start(bf16[384,2048]{1,0:T(8,128)(2,1)} %param.4) | copy-start | bytes 4718596
  7.2 79.1 %all-gather.3.cloned.1.call-start = ((), (), s32[]{:S(2)}) async-start(), calls=%async_computation.1 | async-start | bytes 4718592 | tf_op jit(solution)/shard_map/all_gather | solution.py:18
  9.3 152.8 %all-gather.5.cloned.1.call-start = ((), (), s32[]{:S(2)}) async-start(), calls=%async_computation.2 | async-start | bytes 4718592 | tf_op jit(solution)/shard_map/all_gather | solution.py:19
  11.2 252.7 %reduce-scatter.2.cloned.1.call-start = ((), (), s32[]{:S(2)}) async-start(), calls=%async_computation.4 | async-start | bytes 4718592 | tf_op jit(solution)/shard_map/reduce_scatter | solution.py:30
  11.3 38.3 %collective-permute-start = (bf16[384,2048]{1,0:T(8,128)(2,1)S(1)}, bf16[384,2048]{1,0:T(8,128)(2,1)S(1)}, u32[]{:S(2)}, u32[]{:S(2)}) collective-permute-start(bf16[384,2048]{1,0:T(8,128)(2,1)S(1)} %copy-done.2), channel_id=1, source_target_pairs={{16,0},{0,16},{17,1},{1,17},{18,2},{2,18},{19,3},{3,19},{20,4},{4,... | collective-permute-start | bytes 4718600 | tf_op jit(solution)/shard_map/ppermute | solution.py:14
  14.3 80.2 %collective-permute-start.1 = (bf16[384,2048]{1,0:T(8,128)(2,1)}, bf16[384,2048]{1,0:T(8,128)(2,1)}, u32[]{:S(2)}, u32[]{:S(2)}) collective-permute-start(bf16[384,2048]{1,0:T(8,128)(2,1)} %param.7), channel_id=1, source_target_pairs={{16,0},{0,16},{17,1},{1,17},{18,2},{2,18},{19,3},{3,19},{20,4},{4,... | collective-permute-start | bytes 4718600 | tf_op jit(solution)/shard_map/ppermute | solution.py:14
  50.8 111.3 %copy-start.3 = (bf16[384,2048]{1,0:T(8,128)(2,1)S(1)}, bf16[384,2048]{1,0:T(8,128)(2,1)}, u32[]{:S(2)}) copy-start(bf16[384,2048]{1,0:T(8,128)(2,1)} %param.7) | copy-start | bytes 4718596
  169.1 1.1 copy-start.4
  177.3 1.4 copy-start.5
  177.4 109.4 %all-reduce.2.cloned.1.call-start = ((), (), s32[]{:S(2)}) async-start(), calls=%async_computation.3 | async-start | bytes 3145728 | tf_op jit(solution)/shard_map/psum | solution.py:38
  184.2 35.5 %collective-permute-start.2 = (bf16[384,2048]{1,0:T(8,128)(2,1)S(1)}, bf16[384,2048]{1,0:T(8,128)(2,1)S(1)}, u32[]{:S(2)}, u32[]{:S(2)}) collective-permute-start(bf16[384,2048]{1,0:T(8,128)(2,1)S(1)} %slice.15), channel_id=1, source_target_pairs={{16,0},{0,16},{17,1},{1,17},{18,2},{2,18},{19,3},{3,19},{20,4},{4,... | collective-permute-start | bytes 4718600 | tf_op jit(solution)/shard_map/ppermute | solution.py:14
  263.9 13.6 %collective-permute-start.3 = (bf16[256,1024]{1,0:T(8,128)(2,1)}, bf16[256,1024]{1,0:T(8,128)(2,1)}, u32[]{:S(2)}, u32[]{:S(2)}) collective-permute-start(bf16[256,1024]{1,0:T(8,128)(2,1)} %reduce-scatter.2.cloned.1.call-done), channel_id=1, source_target_pairs={{16,0},{0,16},{17,1},{1,17},{18,2},{2,18},{19,3},{3,19},{20,4},{4,... | collective-permute-start | bytes 1572872 | tf_op jit(solution)/shard_map/ppermute | solution.py:14
  278.7 10.8 %copy-start.1 = (f32[256,2048]{1,0:T(8,128)}, f32[256,2048]{1,0:T(8,128)S(1)}, u32[]{:S(2)}) copy-start(f32[256,2048]{1,0:T(8,128)S(1)} %convert_dynamic-update-slice_fusion) | copy-start | bytes 6291460
Sparse Core Ops, SparseCore 0:
  10.7 75.5 all-gather.2
  88.9 73.1 all-gather.4
  177.5 86.4 reduce-scatter.1
  266.7 19.9 all-reduce.1

commit v2 on v0

v2 whole, which is shorter than its diff:
```python
import functools

import jax
import jax.numpy as jnp
from jax import lax
from jax.experimental import pallas as pl
from jax.experimental.pallas import tpu as pltpu
from jax.sharding import PartitionSpec as P

MESH = pl.DeviceIdType.MESH


def gather_kernel(line, x_ref, c_ref, w_ref, wall_ref, tx_ref, tc_ref, zs, zr, ys, yr, ts, tr, cs, cr):
    r, f, c = lax.axis_index("rep"), lax.axis_index("fs"), lax.axis_index("tp")
    p, at = lax.rem(f, 2), lax.div(f, 2)
    core = lax.rem(c, 2)
    f_other = f + 1 - 2 * p
    to_x, to_y, to_core = {"rep": 1 - r}, {"fs": f_other}, {"tp": c + 1 - 2 * core}
    up, down = {"fs": f + 2}, {"fs": f - 2}
    has_up, has_down = at < line - 1, at > 0

    barrier = pltpu.get_barrier_semaphore()
    for dev in (to_x, to_y, to_core):
        pl.semaphore_signal(barrier, inc=1, device_id=dev, device_id_type=MESH)

    @pl.when(has_up)
    def _():
        pl.semaphore_signal(barrier, inc=1, device_id=up, device_id_type=MESH)

    @pl.when(has_down)
    def _():
        pl.semaphore_signal(barrier, inc=1, device_id=down, device_id_type=MESH)

    inner = has_up & has_down

    @pl.when(inner)
    def _():
        pl.semaphore_wait(barrier, 5)

    @pl.when(jnp.logical_not(inner))
    def _():
        pl.semaphore_wait(barrier, 4 if line > 1 else 3)

    def remote(src, dst, send, recv, dev):
        return pltpu.make_async_remote_copy(
            src_ref=src, dst_ref=dst, send_sem=send, recv_sem=recv, device_id=dev, device_id_type=MESH
        )

    half = x_ref.shape[0] // 2
    mine = pl.ds(pl.multiple_of(core * half, half), half)
    theirs = pl.ds(pl.multiple_of((1 - core) * half, half), half)
    toks = (tx_ref, tc_ref)

    y_copy = remote(w_ref.at[1 - p], wall_ref.at[:, f], ys, yr, to_y)
    y_copy.start()

    def z_copy(go_up, s, j):
        owner = (at - s if go_up else at + s) * 2 + (p if j == 0 else 1 - p)
        src = w_ref.at[p] if (s == 0 and j == 0) else wall_ref.at[:, owner]
        d = 0 if go_up else 1
        return remote(src, wall_ref.at[:, owner], zs.at[d, s, j], zr.at[d, s, j], up if go_up else down)

    def valid(go_up, s):
        return ((at - s >= 0) & has_up) if go_up else ((at + s < line) & has_down)

    def arrived(go_up, s):
        return (at - s >= 0) if go_up else (at + s < line)

    def z_step(s, j):
        for go_up in (True, False):
            d = 0 if go_up else 1
            if s > 0:
                @pl.when(arrived(go_up, s))
                def _():
                    owner = (at - s if go_up else at + s) * 2 + (p if j == 0 else 1 - p)
                    blk = wall_ref.at[:, owner]
                    remote(blk, blk, zs.at[d, s - 1, j], zr.at[d, s - 1, j], to_x).wait_recv()
            if s < line - 1:
                @pl.when(valid(go_up, s))
                def _():
                    z_copy(go_up, s, j).start()

    z_step(0, 0)

    own = (x_ref, c_ref)
    x_first = [remote(own[a].at[mine], toks[a].at[0, mine], ts.at[0, a], tr.at[0, a], to_x) for a in (0, 1)]
    y_first = [remote(own[a].at[mine], toks[a].at[1, mine], ts.at[1, a], tr.at[1, a], to_y) for a in (0, 1)]
    x_first[0].start()
    y_first[1].start()
    x_first[1].start()
    y_first[0].start()
    diag = [
        remote(tx_ref.at[0, mine], tx_ref.at[2, mine], ts.at[2, 0], tr.at[2, 0], to_y),
        remote(tc_ref.at[1, mine], tc_ref.at[2, mine], ts.at[2, 1], tr.at[2, 1], to_x),
    ]

    def swap(slot, a):
        return remote(toks[a].at[slot, mine], toks[a].at[slot, mine], cs.at[slot, a], cr.at[slot, a], to_core)

    y_copy.wait_recv()
    z_step(0, 1)

    def tokens_first():
        x_first[0].wait_recv()
        diag[0].start()
        swap(0, 0).start()
        y_first[1].wait_recv()
        diag[1].start()
        swap(1, 1).start()

    def tokens_second():
        x_first[1].wait_recv()
        swap(0, 1).start()
        y_first[0].wait_recv()
        swap(1, 0).start()

    todo = [tokens_first, tokens_second]
    for s in range(1, line):
        for j in (0, 1):
            z_step(s, j)
        if todo:
            todo.pop(0)()
    for more in todo:
        more()
    for a in (0, 1):
        diag[a].wait_recv()
        swap(2, a).start()
    for slot in range(3):
        for a in (0, 1):
            blk = toks[a].at[slot, theirs]
            remote(blk, blk, cs.at[slot, a], cr.at[slot, a], to_core).wait_recv()
    for slot in range(3):
        for a in (0, 1):
            swap(slot, a).wait_send()
    for copy in x_first + y_first + diag + [y_copy]:
        copy.wait_send()
    for s in range(line - 1):
        for j in (0, 1):
            for go_up in (True, False):
                @pl.when(valid(go_up, s))
                def _():
                    z_copy(go_up, s, j).wait_send()


def gather(n_fs, x, c, w):
    line = n_fs // 2
    tokens, width = x.shape
    rows, cols = w.shape[2:]
    dma = pltpu.SemaphoreType.DMA
    hbm = pl.BlockSpec(memory_space=pl.ANY)
    return pl.pallas_call(
        functools.partial(gather_kernel, line),
        out_shape=(
            jax.ShapeDtypeStruct((2, n_fs, rows, cols), w.dtype),
            jax.ShapeDtypeStruct((3, tokens, width), x.dtype),
            jax.ShapeDtypeStruct((3, tokens, width), c.dtype),
        ),
        in_specs=[hbm] * 3,
        out_specs=(hbm,) * 3,
        scratch_shapes=[
            dma((2, line, 2)), dma((2, line, 2)), dma, dma,
            dma((3, 2)), dma((3, 2)), dma((3, 2)), dma((3, 2)),
        ],
        compiler_params=pltpu.CompilerParams(collective_id=0, has_side_effects=True),
    )(x, c, w)


def per_device(inputs, w_up, w_down, cotangent):
    n_rep, n_fs, n_tp = lax.axis_size("rep"), lax.axis_size("fs"), lax.axis_size("tp")
    rep, fs, tp = lax.axis_index("rep"), lax.axis_index("fs"), lax.axis_index("tp")
    pair = lax.rem(fs, 2)
    tokens, width = inputs.shape
    rows, block = w_up.shape
    hq = block // (n_rep * 2)
    f32, bf16 = jnp.float32, jnp.bfloat16

    both = lax.dynamic_slice_in_dim(w_up, rep * 2 * hq, 2 * hq, axis=1)
    both_down = lax.dynamic_slice_in_dim(w_down, rep * 2 * hq, 2 * hq, axis=0)
    w = jnp.stack([both.reshape(rows, 2, hq), both_down.T.reshape(rows, 2, hq)])
    w = w.transpose(2, 0, 1, 3)
    wall, tx, tc = gather(n_fs, inputs, cotangent, w)
    own_w = lax.dynamic_index_in_dim(w, pair, axis=0, keepdims=False)
    wall = lax.dynamic_update_slice(wall, own_w[:, None], (0, fs, 0, 0))
    up = wall[0].reshape(width, hq)
    down = wall[1].reshape(width, hq)
    tx, tc = tx.reshape(3 * tokens, width), tc.reshape(3 * tokens, width)

    def dot(a, b, da, db):
        return lax.dot_general(a, b, (((da,), (db,)), ((), ())), preferred_element_type=f32)

    def grad(x, c):
        return (2.0 * jnp.maximum(dot(x, up, 1, 0), 0.0) * dot(c, down, 1, 0)).astype(bf16)

    g_own, g_far = grad(inputs, cotangent), grad(tx, tc)
    d_w = (dot(inputs, g_own, 0, 0) + dot(tx, g_far, 0, 0)).astype(bf16)
    groups = [[2 * k + j for k in range(n_fs // 2)] for j in range(2)]
    two = lax.psum_scatter(d_w, "fs", scatter_dimension=0, axis_index_groups=groups, tiled=True)

    everyone = [(a, b) for a in range(n_rep) for b in range(n_fs)]

    def quad(value, dr, dp):
        moves = [(a * n_fs + b, ((a + dr) % n_rep) * n_fs + (b ^ dp)) for a, b in everyone]
        return lax.ppermute(value, ("rep", "fs"), moves)

    part = tokens // n_tp
    p_own, p_far = dot(g_own, up, 1, 1), dot(g_far, up, 1, 1)
    whole = jnp.concatenate([p_own[None], p_far.reshape(3, tokens, width)]).astype(bf16)
    whole = whole.reshape(4, n_tp, part, width)

    def tp_from(value, k):
        return lax.ppermute(value, "tp", [((i + k) % n_tp, i) for i in range(n_tp)])

    def part_of(k):
        return lax.dynamic_index_in_dim(whole, lax.rem(tp + k, n_tp), axis=1, keepdims=False)

    total = part_of(0).astype(f32)
    for k in range(1, n_tp):
        total = total + tp_from(part_of(n_tp - k), k).astype(f32)
    acc = total[0]
    for i, (dr, dp) in enumerate([(1, 0), (0, 1), (1, 1)]):
        acc = acc + quad(total[i + 1].astype(bf16), dr, dp).astype(f32)
    acc = acc.astype(bf16)
    d_inputs = jnp.zeros((tokens, width), bf16)
    for k in range(n_tp):
        piece = acc if k == 0 else tp_from(acc, k)
        d_inputs = lax.dynamic_update_slice_in_dim(d_inputs, piece, lax.rem(tp + k, n_tp) * part, axis=0)

    two = two.reshape(2, rows, hq)
    keep = lax.dynamic_index_in_dim(two, pair, axis=0, keepdims=False)
    give = lax.dynamic_index_in_dim(two, 1 - pair, axis=0, keepdims=False)
    d_w_up = jnp.zeros((rows, block), f32)
    for dr in range(n_rep):
        for dp in range(2):
            piece = give if dp else keep
            if dr or dp:
                piece = quad(piece, dr, dp)
            q = lax.rem(rep + dr, n_rep) * 2 + (1 - pair if dp else pair)
            d_w_up = lax.dynamic_update_slice_in_dim(d_w_up, piece.astype(f32), q * hq, axis=1)
    return (d_inputs, d_w_up)


def solution(mesh):
    in_specs = (P(("rep", "fs"), None), P("fs", "tp"), P("tp", "fs"), P(("rep", "fs"), None))
    out_specs = (P(("rep", "fs"), None), P("fs", "tp"))
    return jax.shard_map(
        per_device, mesh=mesh, in_specs=in_specs, out_specs=out_specs, check_vma=False
    )
```

time: 654 us -> 194 us (0.30)
  waiting for transfers between devices: 599 us -> 40.4 us
  Pallas kernels: 0 us -> 78.4 us
  other arithmetic: 0 us -> 17.3 us
  matrix products: 33.1 us -> 21.3 us
  local copies, waits for them, and re-layouts: 7.35 us -> 14.8 us
  starting transfers between devices: 0.19 us -> 7.53 us
    reduce_scatter x1, waiting for transfers between devices: 279 us -> 30.2 us  [per_device(): lax.psum_scatter(d_w, 'fs', scatter_dimension=0, axis_index_groups=groups...]
    all_gather x2 -> x0, waiting for transfers between devices: 245 us -> none  [the longest x1 129 us: per_device(): lax.all_gather(w_down, 'fs', axis=1, tiled=True)]
    pallas_call x0 -> x1, Pallas kernels: none -> 78.4 us  [gather(): pl.pallas_call(functools.partial(gather_kernel, line), out_shape=(jax.Sha...]
    psum x2 -> x0, waiting for transfers between devices: 74.6 us -> none  [the longest x1 54.3 us: per_device(): d_w_up = lax.psum(own_rows, 'rep')]
    dot_general x4 -> x8, matrix products: 33.1 us -> 21.3 us  [dot(): lax.dot_general(a, b, (((da,), (db,)), ((), ())), preferred_element_type=...]
    ppermute x0 -> x8, waiting for transfers between devices: none -> 10.2 us  [the longest x6 10.2 us: quad(): return lax.ppermute(value, ('rep', 'fs'), moves)]
    ppermute x0 -> x8, starting transfers between devices: none -> 7.49 us  [the longest x6 7.11 us: quad(): return lax.ppermute(value, ('rep', 'fs'), moves)]
    another operation x0 -> x1, other arithmetic: none -> 6.75 us
  transfers between devices with their start and end apart: 5 -> 9, of which waited for: 5 -> 2; matrix products, arithmetic and copies ran while one was open for 3% -> 12% of each run, Pallas kernels for 0% -> 0%
where the time goes in v2:
time: 194 us
  Pallas kernels  78.4 us (40%)
  waiting for transfers between devices  40.4 us (21%)
  matrix products  21.3 us (11%)
  other arithmetic  17.3 us (9%)
  local copies, waits for them, and re-layouts  14.8 us (8%)
  between operations  14.4 us (7%)
  starting transfers between devices  7.53 us (4%)
    pallas_call x1, Pallas kernels, gather(): pl.pallas_call(functools.partial(gather_kernel, line), out_shape=(jax.Sha...  78.4 us
    reduce_scatter x1, waiting for transfers between devices, per_device(): lax.psum_scatter(d_w, 'fs', scatter_dimension=0, axis_index_groups=groups...  30.2 us
    dot_general x8, matrix products, dot(): lax.dot_general(a, b, (((da,), (db,)), ((), ())), preferred_element_type=...  21.3 us
    ppermute x6, waiting for transfers between devices, quad(): return lax.ppermute(value, ('rep', 'fs'), moves)  10.2 us
    ppermute x6, starting transfers between devices, quad(): return lax.ppermute(value, ('rep', 'fs'), moves)  7.11 us
    another operation x1, other arithmetic  6.75 us
    unnamed x29, local copies, waits for them, and re-layouts  3.91 us
  transfers between devices with their start and end apart: 9, of which 2 were waited for; matrix products, arithmetic and copies ran while one was open for 12% of the time, Pallas kernels for 0%

profile of v2, /device:TPU:0, one launch (start us, length us, event | category | flops | bytes accessed | tf_op | source)
XLA Modules:
  0.0 194.1 jit_solution(16079859189110070691)
XLA Ops:
  7.3 1.1 copy-done
  10.2 78.4 %shard_map.59 = (bf16[2,8,256,512]{3,2,1,0:T(8,128)(2,1)}, bf16[3,384,2048]{2,1,0:T(8,128)(2,1)}, bf16[3,384,2048]{2,1,0:T(8,128)(2,1)}) custom-call(bf16[384,2048]{1,0:T(8,128)(2,1)} %x_ref.1, bf16[384,2048]{1,0:T(8,128)(2,1)} %c_ref.1, bf16[2,2,256,512]{3,2,1,0:T(8,128)(2,1)} %fusion.14.w_ref), custom_call_target="tpu_custom_call" | custom-call | tf_op jit(solution)/shard_map/pallas_call | solution.py:151
  89.5 3.5 %fusion.20 = (bf16[1,8,256,512]{3,2,1,0:T(8,128)(2,1)S(1)}, bf16[1,8,256,512]{3,2,1,0:T(8,128)(2,1)S(1)}) fusion(bf16[2,8,256,512]{3,2,1,0:T(8,128)(2,1)} %fusion.17), kind=kLoop, calls=%fused_computation.48 | loop fusion | bytes 8388608 | tf_op jit(solution)/shard_map/slice | solution.py:185
  94.0 2.6 %fusion.1 = f32[1152,512]{1,0:T(8,128)S(1)} fusion(bf16[1152,2048]{1,0:T(8,128)(2,1)S(1)} %bitcast.91, bf16[2048,512]{1,0:T(8,128)(2,1)S(1)} %bitcast.79), kind=kOutput, calls=%fused_computation.10 | convolution fusion | flops 2417098752 | bytes 9175040 | tf_op jit(solution)/shard_map/dot_general | solution.py:189
  97.7 2.7 %fusion.6 = bf16[1152,512]{1,0:T(8,128)(2,1)S(1)} fusion(f32[1152,512]{1,0:T(8,128)S(1)} %fusion.1, bf16[1152,2048]{1,0:T(8,128)(2,1)S(1)} %bitcast.94, bf16[2048,512]{1,0:T(8,128)(2,1)S(1)} %bitcast.83), kind=kOutput, calls=%fused_computation.15 | convolution fusion | flops 2417098752 | bytes 10354688 | tf_op jit(solution)/shard_map/dot_general | solution.py:189
  100.4 2.2 %fusion.7 = bf16[1,2,192,2048]{3,2,1,0:T(8,128)(2,1)} fusion(bf16[2,192,512]{2,1,0:T(8,128)(2,1)S(1)} %bitcast.85, bf16[2048,512,1]{1,0,2:T(8,128)(2,1)S(1)} %bitcast.80), kind=kOutput, calls=%fused_computation.17 | convolution fusion | flops 806092800 | bytes 4063232 | tf_op jit(solution)/shard_map/dot_general | solution.py:189
  102.6 4.3 %convolution_convert_fusion = bf16[3,2,192,2048]{3,2,1,0:T(8,128)(2,1)} fusion(bf16[3,2,192,512]{3,2,1,0:T(8,128)(2,1)S(1)} %bitcast.95, bf16[2048,512,1,1]{1,0,3,2:T(8,128)(2,1)S(1)} %bitcast.81), kind=kOutput, calls=%fused_computation.7 | convolution fusion | flops 2418278400 | bytes 7995392 | tf_op jit(solution)/shard_map/dot_general | solution.py:189
  106.9 3.8 %fusion.3 = bf16[4,192,2048]{2,1,0:T(8,128)(2,1)} fusion(s32[]{:T(128)S(6)} %select_n.45, bf16[3,2,192,2048]{3,2,1,0:T(8,128)(2,1)} %convolution_convert_fusion, bf16[1,2,192,2048]{3,2,1,0:T(8,128)(2,1)} %fusion.7), kind=kLoop, calls=%fused_computation.12 | loop fusion | flops 1572864 | bytes 9437188 | tf_op jit(solution)/shard_map/jit(dynamic_index_in_dim)/squeeze | solution.py:214
  111.1 4.9 %fusion.21 = f32[2048,512]{0,1:T(8,128)S(1)} fusion(bf16[1152,2048]{1,0:T(8,128)(2,1)} %bitcast.88, bf16[1152,512]{1,0:T(8,128)(2,1)S(1)} %copy-done.9), kind=kOutput, calls=%fused_computation.49 | convolution fusion | flops 2415919104 | bytes 10092544 | tf_op jit(solution)/shard_map/dot_general | solution.py:189
  116.0 2.7 %fusion = bf16[2048,512]{0,1:T(8,128)(2,1)} fusion(f32[2048,512]{0,1:T(8,128)S(1)} %fusion.21, bf16[512,384]{0,1:T(8,128)(2,1)S(1)} %fusion.13, bf16[384,2048]{1,0:T(8,128)(2,1)S(1)} %copy-done.2), kind=kOutput, calls=%fused_computation.6 | convolution fusion | flops 807403520 | bytes 8257536 | tf_op jit(solution)/shard_map/dot_general | solution.py:189
  118.7 1.4 copy-done.3
  120.1 6.8 %fusion.19 = (bf16[4,192,2048]{2,1,0:T(8,128)(2,1)S(1)}, f32[4,192,2048]{2,1,0:T(8,128)}) fusion(bf16[4,192,2048]{2,1,0:T(8,128)(2,1)} %collective-permute-done, s32[]{:T(128)S(6)} %select_n.44, bf16[3,2,192,2048]{3,2,1,0:T(8,128)(2,1)} %convolution_convert_fusion, bf16[1,2,192,2048]{3,2,1,0:T(8,128)(2,1)S(1)} %copy-done.3), kind=kLoop, calls=%fused_computation.47 | loop fusion | flops 7864320 | bytes 18874372 | tf_op jit(solution)/shard_map/convert.3
  126.8 1.1 slice_bitcast_fusion.3
  127.9 1.5 collective-permute-start.1
  129.9 1.5 collective-permute-start.3
  131.4 30.2 %reduce-scatter.2.cloned.1.call-done = bf16[512,512]{0,1:T(8,128)(2,1)} async-done(((bf16[2048,512]{0,1:T(8,128)(2,1)}), bf16[512,512]{0,1:T(8,128)(2,1)}) %reduce-scatter.2.cloned.1.call-update) | async-done | bytes 524304 | tf_op jit(solution)/shard_map/reduce_scatter | solution.py:197
  161.6 1.2 reshape.39
  162.8 1.1 constant_dynamic-slice_fusion
  164.6 1.6 collective-permute-start.5
  166.3 3.5 %constant_dynamic-update-slice_fusion.1 = (bf16[384,2048]{1,0:T(8,128)(2,1)S(1)}, bf16[192,2048]{1,0:T(8,128)(2,1)}) fusion(bf16[384,2048]{1,0:T(8,128)(2,1)S(1)} %broadcast_in_dim.10, s32[]{:T(128)S(6)} %select_n.46, bf16[192,2048]{1,0:T(8,128)(2,1)} %collective-permute-done.3, bf16[192,2048]{1,0:T(8,128)(2,1)} %collective-permute-done.2, ...), kind=kLoop, calls=%fused_computation.44 | loop fusion | flops 2752512 | bytes 5505028 | tf_op jit(solution)/shard_map/dynamic_update_slice | solution.py:226
  169.9 1.5 collective-permute-start.7
  174.0 10.2 %collective-permute-done.6 = bf16[256,512]{1,0:T(8,128)(2,1)S(1)} collective-permute-done((bf16[256,512]{1,0:T(8,128)(2,1)S(1)}, bf16[256,512]{1,0:T(8,128)(2,1)S(1)}, u32[]{:S(2)}, u32[]{:S(2)}) %collective-permute-start.6) | collective-permute-done | bytes 262176 | tf_op jit(solution)/shard_map/ppermute | solution.py:203
  184.3 1.8 constant_dynamic-update-slice_fusion
  186.2 1.1 copy-done.5
  (57 shorter events, 9.3 us)
Async XLA Ops:
  7.2 1.2 copy-start
  7.2 1.7 copy-start.7
  7.2 154.4 %reduce-scatter.2.cloned.1.call-start = ((), (), s32[]{:S(2)}) async-start(), calls=%async_computation.1 | async-start | bytes 2621440 | tf_op jit(solution)/shard_map/reduce_scatter | solution.py:197
  88.6 5.4 %slice-start = ((s8[4718592]{0:T(1024)(128)(4,1)}), s8[4194304]{0:T(1024)(128)(4,1)S(1)}, s32[]{:S(2)}) async-start(s8[4718592]{0:T(1024)(128)(4,1)} %bitcast.89), calls=%async_computation.2 | async-start | bytes 8388608
  89.5 3.5 %copy-start.2 = (bf16[384,2048]{1,0:T(8,128)(2,1)S(1)}, bf16[384,2048]{1,0:T(8,128)(2,1)}, u32[]{:S(2)}) copy-start(bf16[384,2048]{1,0:T(8,128)(2,1)} %x_ref.1) | copy-start | bytes 4718596
  89.5 4.5 %slice-start.1 = ((s8[4718592]{0:T(1024)(128)(4,1)}), s8[524288]{0:T(1024)(128)(4,1)S(1)}, s32[]{:S(2)}) async-start(s8[4718592]{0:T(1024)(128)(4,1)} %bitcast.89), calls=%async_computation.3 | async-start | bytes 1048576
  93.0 4.7 %slice-start.2 = ((s8[4718592]{0:T(1024)(128)(4,1)}), s8[4194304]{0:T(1024)(128)(4,1)S(1)}, s32[]{:S(2)}) async-start(s8[4718592]{0:T(1024)(128)(4,1)} %bitcast.92), calls=%async_computation.4 | async-start | bytes 8388608
  94.0 2.6 %copy-start.6 = (bf16[384,2048]{1,0:T(8,128)(2,1)S(1)}, bf16[384,2048]{1,0:T(8,128)(2,1)}, u32[]{:S(2)}) copy-start(bf16[384,2048]{1,0:T(8,128)(2,1)} %c_ref.1) | copy-start | bytes 4718596
  94.0 3.7 %slice-start.3 = ((s8[4718592]{0:T(1024)(128)(4,1)}), s8[524288]{0:T(1024)(128)(4,1)S(1)}, s32[]{:S(2)}) async-start(s8[4718592]{0:T(1024)(128)(4,1)} %bitcast.92), calls=%async_computation.5 | async-start | bytes 1048576
  100.4 2.2 %copy-start.8 = (bf16[1152,512]{1,0:T(8,128)(2,1)}, bf16[1152,512]{1,0:T(8,128)(2,1)S(1)}, u32[]{:S(2)}) copy-start(bf16[1152,512]{1,0:T(8,128)(2,1)S(1)} %fusion.6) | copy-start | bytes 3538948
  106.9 4.2 %copy-start.9 = (bf16[1152,512]{1,0:T(8,128)(2,1)S(1)}, bf16[1152,512]{1,0:T(8,128)(2,1)}, u32[]{:S(2)}) copy-start(bf16[1152,512]{1,0:T(8,128)(2,1)} %copy-done.8) | copy-start | bytes 3538948
  110.7 8.0 %collective-permute-start = (bf16[4,192,2048]{2,1,0:T(8,128)(2,1)}, bf16[4,192,2048]{2,1,0:T(8,128)(2,1)}, u32[]{:S(2)}, u32[]{:S(2)}) collective-permute-start(bf16[4,192,2048]{2,1,0:T(8,128)(2,1)} %fusion.3), channel_id=1, source_target_pairs={{1,0},{0,1},{3,2},{2,3},{5,4},{4,5},{7,6},{6,7},{9,8},{8,9},{11,10... | collective-permute-start | bytes 9437192 | tf_op jit(solution)/shard_map/ppermute | solution.py:211
  118.7 1.4 copy-start.3
  127.9 38.2 %collective-permute-start.1 = (bf16[192,2048]{1,0:T(8,128)(2,1)}, bf16[192,2048]{1,0:T(8,128)(2,1)}, u32[]{:S(2)}, u32[]{:S(2)}) collective-permute-start(bf16[192,2048]{1,0:T(8,128)(2,1)} %get-tuple-element.14), channel_id=1, source_target_pairs={{0,16},{2,18},{4,20},{6,22},{8,24},{10,26},{12,28},{14,30},{16,0},... | collective-permute-start | bytes 2359304 | tf_op jit(solution)/shard_map/ppermute | solution.py:203
  129.4 36.7 %collective-permute-start.2 = (bf16[192,2048]{1,0:T(8,128)(2,1)S(1)}, bf16[192,2048]{1,0:T(8,128)(2,1)}, u32[]{:S(2)}, u32[]{:S(2)}) collective-permute-start(bf16[192,2048]{1,0:T(8,128)(2,1)S(1)} %get-tuple-element.16), channel_id=1, source_target_pairs={{0,2},{2,0},{4,6},{6,4},{8,10},{10,8},{12,14},{14,12},{16,18},{18,... | collective-permute-start | bytes 2359304 | tf_op jit(solution)/shard_map/ppermute | solution.py:203
  129.9 36.2 %collective-permute-start.3 = (bf16[192,2048]{1,0:T(8,128)(2,1)S(1)}, bf16[192,2048]{1,0:T(8,128)(2,1)}, u32[]{:S(2)}, u32[]{:S(2)}) collective-permute-start(bf16[192,2048]{1,0:T(8,128)(2,1)S(1)} %get-tuple-element.15), channel_id=1, source_target_pairs={{0,18},{2,16},{4,22},{6,20},{8,26},{10,24},{12,30},{14,28},{16,2},... | collective-permute-start | bytes 2359304 | tf_op jit(solution)/shard_map/ppermute | solution.py:203
  164.6 8.3 %collective-permute-start.5 = (bf16[256,512]{1,0:T(8,128)(2,1)S(1)}, bf16[256,512]{1,0:T(8,128)(2,1)}, u32[]{:S(2)}, u32[]{:S(2)}) collective-permute-start(bf16[256,512]{1,0:T(8,128)(2,1)S(1)} %bitcast.86), channel_id=1, source_target_pairs={{0,2},{2,0},{4,6},{6,4},{8,10},{10,8},{12,14},{14,12},{16,18},{18,... | collective-permute-start | bytes 786440 | tf_op jit(solution)/shard_map/ppermute | solution.py:203
  169.9 14.5 %collective-permute-start.4 = (bf16[192,2048]{1,0:T(8,128)(2,1)}, bf16[192,2048]{1,0:T(8,128)(2,1)}, u32[]{:S(2)}, u32[]{:S(2)}) collective-permute-start(bf16[192,2048]{1,0:T(8,128)(2,1)} %get-tuple-element.9), channel_id=1, source_target_pairs={{1,0},{0,1},{3,2},{2,3},{5,4},{4,5},{7,6},{6,7},{9,8},{8,9},{11,10... | collective-permute-start | bytes 2359304 | tf_op jit(solution)/shard_map/ppermute | solution.py:211
  169.9 14.4 %collective-permute-start.7 = (bf16[256,512]{1,0:T(8,128)(2,1)S(1)}, bf16[256,512]{1,0:T(8,128)(2,1)S(1)}, u32[]{:S(2)}, u32[]{:S(2)}) collective-permute-start(bf16[256,512]{1,0:T(8,128)(2,1)S(1)} %bitcast.87), channel_id=1, source_target_pairs={{0,18},{2,16},{4,22},{6,20},{8,26},{10,24},{12,30},{14,28},{16,2},... | collective-permute-start | bytes 786440 | tf_op jit(solution)/shard_map/ppermute | solution.py:203
  172.0 12.2 %collective-permute-start.6 = (bf16[256,512]{1,0:T(8,128)(2,1)S(1)}, bf16[256,512]{1,0:T(8,128)(2,1)S(1)}, u32[]{:S(2)}, u32[]{:S(2)}) collective-permute-start(bf16[256,512]{1,0:T(8,128)(2,1)S(1)} %bitcast.84), channel_id=1, source_target_pairs={{0,16},{2,18},{4,20},{6,22},{8,24},{10,26},{12,28},{14,30},{16,0},... | collective-permute-start | bytes 786440 | tf_op jit(solution)/shard_map/ppermute | solution.py:203
  172.8 14.4 %copy-start.1 = (bf16[256,2048]{1,0:T(8,128)(2,1)S(1)}, bf16[256,2048]{1,0:T(8,128)(2,1)}, u32[]{:S(2)}) copy-start(bf16[256,2048]{1,0:T(8,128)(2,1)} %param.5) | copy-start | bytes 3145732
  184.3 1.8 copy-start.4
  186.1 1.1 copy-start.5
Sparse Core Ops, SparseCore 0:
  118.8 42.7 reduce-scatter.1
